TPU v7x, 512 devices: a whole 4x4x16 slice. The times are simulated.
512 devices in a mesh: fs: 64 (over z, y), tp: 8 (over x, core).
Axes of the slice: x: 4, y: 4, z: 16, core: 2. Of those that a mesh axis runs over, the one named last changes fastest.
Arguments:
- tokens: bfloat16 [49152, 2048], P('fs'), may hold values from -6 to 6
- norm_gain: float32 [2048], replicated, may hold values from 0.1 to 1.9
- gate_weight: float32 [2048, 5120], P('fs', 'tp'), may hold values from -0.125 to 0.125
- value_weight: float32 [2048, 5120], P('fs', 'tp'), may hold values from -0.125 to 0.125
- gate_scale: float32 [5120], P('tp'), may hold values from 0.3 to 3
- value_scale: float32 [5120], P('tp'), may hold values from 0.3 to 3
- gate_kernel: float32 [3, 5120], P(None, 'tp'), may hold values from -3.5 to 3.5
- value_kernel: float32 [3, 5120], P(None, 'tp'), may hold values from -3.5 to 3.5
- gate_bias: float32 [5120], P('tp'), may hold values from -3 to 3
- value_bias: float32 [5120], P('tp'), may hold values from -3 to 3
- down_weight: float32 [5120, 2048], P('tp', 'fs'), may hold values from -0.078125 to 0.078125
- down_scale: float32 [2048], P('tp'), may hold values from 0.3 to 3
Outputs:
- mixed: bfloat16 [49152, 2048], P('fs', 'tp')
All inputs are finite; a program needn't handle non-finite values.
Results may differ from a plain program's by a relative error of at most 0.014.
Values may be sent and summed in bfloat16 or wider, within the bound.
No kernel may reach another device: no remote copies, remote signals or barrier semaphores. Data moves between devices by JAX's collectives and lax.ppermute only.
A program may use at most 64 MiB of HBM per device.

v0:
```python
import jax
import jax.numpy as jnp
from jax import lax
from jax.experimental.layout import Layout, with_layout_constraint
from jax.sharding import Mesh, PartitionSpec as P

epsilon = 1e-06
up_lift = 2.0**17
down_lift = 2.0**19


def down_half(hidden, rows, core):
    groups, _, part, total = rows.shape
    units = hidden.shape[1]
    mine = lax.dynamic_slice(rows, (0, core, 0, total - units), (groups, 1, part, units))
    mine = mine.reshape(groups * part, units).astype(jnp.bfloat16)
    product = lax.dot_general(
        mine, hidden, (((1,), (1,)), ((), ())), preferred_element_type=jnp.float32
    )
    return product.reshape(groups, part, -1)


def causal_mix(current, previous, kernel, tap_bias):
    row_count = current.shape[0]
    joined = jnp.concatenate([previous, current], axis=0).astype(jnp.float32)
    summed_taps = tap_bias[None, :] + kernel[2][None, :] * joined[2:]
    for back_by in (1, 2):
        summed_taps = (
            summed_taps
            + kernel[2 - back_by][None, :] * joined[2 - back_by : 2 - back_by + row_count]
        )
    return summed_taps


def body(
    tokens,
    norm_gain,
    gate_weight,
    value_weight,
    gate_scale,
    value_scale,
    gate_kernel,
    value_kernel,
    gate_bias,
    value_bias,
    down_weight,
    down_scale,
):
    z_count, y_count = (lax.axis_size("z"), lax.axis_size("y"))
    x_count, c_count = (lax.axis_size("x"), lax.axis_size("c"))
    place = lax.axis_index("z") * y_count + lax.axis_index("y")
    core = lax.axis_index("c")
    row_count, width = tokens.shape
    piece, units = gate_weight.shape
    gain = lax.dynamic_slice(norm_gain, (place * piece,), (piece,))[:, None] * up_lift
    shard = jnp.concatenate(
        [gate_weight * gain, value_weight * gain, down_weight.T * down_lift], axis=1
    ).astype(jnp.float16)
    over_z = lax.all_gather(shard, "z", axis=0)
    full = lax.all_gather(over_z, "y", axis=1, tiled=True).reshape(width, 3 * units)
    tokens, full = lax.optimization_barrier((tokens, full))
    values = tokens.astype(jnp.float32)
    factor = lax.rsqrt(jnp.mean(values * values, axis=1, keepdims=True) + epsilon) / up_lift
    pre = []
    for at, scale in ((0, gate_scale), (units, value_scale)):
        raw = jnp.dot(
            tokens,
            full[:, at : at + units].astype(jnp.bfloat16),
            preferred_element_type=jnp.float32,
        )
        pre.append((raw * (factor * scale[None, :])).astype(jnp.bfloat16))
    tails = jnp.concatenate([p[row_count - 2 :] for p in pre], axis=1)
    previous = lax.ppermute(
        tails, ("z", "y"), [(source, source + 1) for source in range(z_count * y_count - 1)]
    )
    gate_conv = causal_mix(pre[0], previous[:, :units], gate_kernel, gate_bias)
    value_conv = causal_mix(pre[1], previous[:, units:], value_kernel, value_bias)
    hidden = (jax.nn.gelu(gate_conv, approximate=True) * value_conv).astype(jnp.bfloat16)
    hidden = with_layout_constraint(hidden, Layout(major_to_minor=(0, 1)))
    rows = full.reshape(x_count, c_count, width // (x_count * c_count), 3 * units)
    sent = down_half(hidden, rows, 1 - core).astype(jnp.bfloat16)
    received = lax.ppermute(sent, "c", [(0, 1), (1, 0)])
    kept = lax.optimization_barrier(down_half(hidden, rows, core))
    paired = (kept + received.astype(jnp.float32)).astype(jnp.bfloat16)
    last_scale, paired = lax.optimization_barrier((down_scale / down_lift, paired))
    parts = lax.all_to_all(paired, "x", 0, 0)
    summed = jnp.sum(parts.astype(jnp.float32), axis=0) * last_scale[:, None]
    return summed.astype(jnp.bfloat16).T


def solution(mesh):
    grid = Mesh(mesh.devices.reshape(16, 4, 4, 2), ("z", "y", "x", "c"))
    fs, tp = (("z", "y"), ("x", "c"))
    return jax.shard_map(
        body,
        mesh=grid,
        in_specs=(
            P(fs, None),
            P(),
            P(fs, tp),
            P(fs, tp),
            P(tp),
            P(tp),
            P(None, tp),
            P(None, tp),
            P(tp),
            P(tp),
            P(tp, fs),
            P(tp),
        ),
        out_specs=P(fs, tp),
        check_vma=False,
    )
```

profile of v0, /device:TPU:32, one launch (start us, length us, event | category | flops | bytes accessed | tf_op | source)
XLA Modules:
  0.0 164.0 jit_solution(14825666330794606886)
XLA Ops:
  0.0 0.9 fusion.37
  0.9 0.8 dynamic-slice_multiply_fusion
  1.7 1.0 fusion.35
  2.7 46.4 %all-gather.2 = f16[16,32,1920]{2,1,0:T(8,128)(2,1)S(1)} all-gather(f16[1,32,1920]{2,1,0:T(8,128)(2,1)S(1)} %pad_maximum_fusion), channel_id=1, replica_groups=mesh['z'=16,'y'=4,'x'=4,'c'=2] {'z'}, dimensions={0}, use_global_device_ids=true | all-gather | bytes 2088960 | tf_op jit(solution)/shard_map/all_gather | solution.py:59
  49.2 61.7 %all-gather.3 = f16[16,128,1920]{2,1,0:T(8,128)(2,1)S(1)} all-gather(f16[16,32,1920]{2,1,0:T(8,128)(2,1)S(1)} %all-gather.2), channel_id=1, replica_groups=mesh['z'=16,'y'=4,'x'=4,'c'=2] {'y'}, dimensions={1}, use_global_device_ids=true | all-gather | bytes 9830400 | tf_op jit(solution)/shard_map/all_gather | solution.py:60
  110.9 0.0 copy-done.1
  110.9 0.7 multiply_reduce_fusion
  111.6 0.0 copy-done.7
  111.6 0.0 copy-start.8
  111.6 2.6 %multiply_convert_fusion = bf16[768,640]{1,0:T(8,128)(2,1)S(1)} fusion(bf16[768,2048]{1,0:T(8,128)(2,1)S(1)} %copy-done.1, f16[2048,1920]{1,0:T(8,128)(2,1)S(1)} %bitcast.35, f32[640]{0:T(1024)S(1)} %copy-done.7, f32[768]{0:T(1024)S(1)} %rsqrt_multiply_fusion), kind=kOutput, calls=%fused_computation.31 | convolution fusion | flops 2016051200 | bytes 6758400 | tf_op jit(solution)/shard_map/dot_general | solution.py:66
  114.2 0.0 copy-done
  114.2 0.0 copy-done.8
  114.2 0.0 copy-start.2
  114.3 0.0 copy-start.3
  114.3 2.6 %multiply_convert_fusion.1 = bf16[768,640]{1,0:T(8,128)(2,1)S(1)} fusion(bf16[768,2048]{1,0:T(8,128)(2,1)S(1)} %copy-done.1, f16[2048,1920]{1,0:T(8,128)(2,1)S(1)} %bitcast.36, f32[640]{0:T(1024)S(1)} %copy-done.8, f32[768]{0:T(1024)S(1)} %rsqrt_multiply_fusion), kind=kOutput, calls=%fused_computation.32 | convolution fusion | flops 2016051200 | bytes 6758400 | tf_op jit(solution)/shard_map/dot_general | solution.py:66
  116.9 3.2 %collective-permute-start = (bf16[2,1280]{1,0:T(2,128)(2,1)S(1)}, bf16[2,1280]{1,0:T(2,128)(2,1)S(1)}, u32[]{:S(2)}, u32[]{:S(2)}) collective-permute-start(bf16[2,1280]{1,0:T(2,128)(2,1)S(1)} %pad_maximum_fusion.1), channel_id=1, source_target_pairs={{0,8},{8,16},{16,24},{24,32},{32,40},{40,48},{48,56},{56,64},{64,7... | collective-permute-start | bytes 15368 | tf_op jit(solution)/shard_map/ppermute | solution.py:73
  120.2 4.8 %collective-permute-done = bf16[2,1280]{1,0:T(2,128)(2,1)S(1)} collective-permute-done((bf16[2,1280]{1,0:T(2,128)(2,1)S(1)}, bf16[2,1280]{1,0:T(2,128)(2,1)S(1)}, u32[]{:S(2)}, u32[]{:S(2)}) %collective-permute-start) | collective-permute-done | bytes 5152 | tf_op jit(solution)/shard_map/ppermute | solution.py:73
  125.0 0.0 copy-start.5
  125.0 0.4 maximum_convert_fusion
  125.4 0.3 copy-done.4
  125.7 0.0 copy-done.5
  125.7 2.0 %fusion.14 = bf16[768,640]{1,0:T(8,128)(2,1)S(1)} fusion(f32[770,640]{1,0:T(8,128)S(1)} %get-tuple-element.24, f32[770,640]{1,0:T(8,128)S(1)} %get-tuple-element.23, f32[640]{0:T(1024)S(1)} %get-tuple-element.17, f32[640]{0:T(1024)S(1)} %get-tuple-element.18, f32[640]{0:T(1024)S(1)} %get-tuple-element.16, f32[640]{0:T(1024)S(1)} %copy-done.4, ...), kind=kLoop, calls=%fused_computation.18 | loop fusion | flops 10813440 | bytes 12800000 | tf_op jit(solution)/shard_map/convert_element_type | solution.py:78
  127.7 0.0 copy-start.6
  127.7 4.0 %convolution_convert_fusion = bf16[4,256,768]{2,1,0:T(8,128)(2,1)} fusion(f16[4,2,256,1920]{3,2,1,0:T(8,128)(2,1)} %bitcast.37, s32[]{:T(128)S(6)} %select_n.11, bf16[768,640]{1,0:T(8,128)(2,1)S(1)} %fusion.14), kind=kOutput, calls=%fused_computation.33 | convolution fusion | flops 1008074752 | bytes 3866628 | tf_op jit(solution)/shard_map/dot_general | solution.py:17
  131.7 1.9 %collective-permute-start.1 = (bf16[4,256,768]{2,1,0:T(8,128)(2,1)}, bf16[4,256,768]{2,1,0:T(8,128)(2,1)S(1)}, u32[]{:S(2)}, u32[]{:S(2)}) collective-permute-start(bf16[4,256,768]{2,1,0:T(8,128)(2,1)} %convolution_convert_fusion), channel_id=1, source_target_pairs={{0,1},{1,0},{2,3},{3,2},{4,5},{5,4},{6,7},{7,6},{8,9},{9,8},{10,11... | collective-permute-start | bytes 4718600 | tf_op jit(solution)/shard_map/ppermute | solution.py:82
  133.6 2.8 %fusion.28 = f32[4,256,768]{2,1,0:T(8,128)S(1)} fusion(f16[4,2,256,1920]{3,2,1,0:T(8,128)(2,1)} %bitcast.38, s32[]{:T(128)S(6)} %select_n.10, bf16[768,640]{1,0:T(8,128)(2,1)S(1)} %fusion.14), kind=kOutput, calls=%fused_computation.38 | convolution fusion | flops 1007288320 | bytes 5439492 | tf_op jit(solution)/shard_map/dot_general | solution.py:17
  136.4 0.8 collective-permute-done.1
  137.2 0.4 add_convert_fusion
  137.7 25.1 %all_to_all.5 = bf16[4,256,768]{2,1,0:T(8,128)(2,1)S(1)} all-to-all(bf16[4,256,768]{2,1,0:T(8,128)(2,1)S(1)} %add_convert_fusion), channel_id=1, replica_groups=mesh['z'=16,'y'=4,'x'=4,'c'=2] {'x'}, dimensions={0} | all-to-all | bytes 3145728 | tf_op jit(solution)/shard_map/all_to_all | solution.py:86
  162.8 0.2 convert_reduce_fusion
  163.0 0.1 fusion.34
  163.1 0.9 copy.17
  (15 shorter events, 0.1 us)
Async XLA Ops:
  49.2 61.7 %copy-start.1 = (bf16[768,2048]{1,0:T(8,128)(2,1)S(1)}, bf16[768,2048]{1,0:T(8,128)(2,1)}, u32[]{:S(2)}) copy-start(bf16[768,2048]{1,0:T(8,128)(2,1)} %param.12) | copy-start | bytes 9437188
  110.9 3.4 %copy-start = (f16[16,128,1920]{2,1,0:T(8,128)(2,1)}, f16[16,128,1920]{2,1,0:T(8,128)(2,1)S(1)}, u32[]{:S(2)}) copy-start(f16[16,128,1920]{2,1,0:T(8,128)(2,1)S(1)} %all-gather.3) | copy-start | bytes 23592964
  110.9 0.7 copy-start.7
  111.6 2.7 %copy-start.8 = (f32[640]{0:T(1024)S(1)}, f32[640]{0:T(1024)}, u32[]{:S(2)}) copy-start(f32[640]{0:T(1024)} %param.16) | copy-start | bytes 7684
  114.2 5.9 %copy-start.2 = (f32[3,640]{1,0:T(4,128)S(1)}, f32[3,640]{1,0:T(4,128)}, u32[]{:S(2)}) copy-start(f32[3,640]{1,0:T(4,128)} %param.19) | copy-start | bytes 23044
  114.3 5.9 %copy-start.3 = (f32[3,640]{1,0:T(4,128)S(1)}, f32[3,640]{1,0:T(4,128)}, u32[]{:S(2)}) copy-start(f32[3,640]{1,0:T(4,128)} %param.18) | copy-start | bytes 23044
  116.9 8.0 %collective-permute-start = (bf16[2,1280]{1,0:T(2,128)(2,1)S(1)}, bf16[2,1280]{1,0:T(2,128)(2,1)S(1)}, u32[]{:S(2)}, u32[]{:S(2)}) collective-permute-start(bf16[2,1280]{1,0:T(2,128)(2,1)S(1)} %pad_maximum_fusion.1), channel_id=1, source_target_pairs={{0,8},{8,16},{16,24},{24,32},{32,40},{40,48},{48,56},{56,64},{64,7... | collective-permute-start | bytes 15368 | tf_op jit(solution)/shard_map/ppermute | solution.py:73
  125.0 0.7 copy-start.4
  125.0 0.7 copy-start.5
  127.7 5.9 %copy-start.6 = (f32[256]{0:T(256)S(1)}, f32[256]{0:T(256)}, u32[]{:S(2)}) copy-start(f32[256]{0:T(256)} %param.23) | copy-start | bytes 3076
  131.7 5.5 %collective-permute-start.1 = (bf16[4,256,768]{2,1,0:T(8,128)(2,1)}, bf16[4,256,768]{2,1,0:T(8,128)(2,1)S(1)}, u32[]{:S(2)}, u32[]{:S(2)}) collective-permute-start(bf16[4,256,768]{2,1,0:T(8,128)(2,1)} %convolution_convert_fusion), channel_id=1, source_target_pairs={{0,1},{1,0},{2,3},{3,2},{4,5},{5,4},{6,7},{7,6},{8,9},{9,8},{10,11... | collective-permute-start | bytes 4718600 | tf_op jit(solution)/shard_map/ppermute | solution.py:82
where the time goes:
time: 164 us
  blocking collectives  133 us (81%)
  matrix products  12 us (7%)
  other arithmetic  6.59 us (4%)
  waiting for transfers between devices  5.54 us (3%)
  starting transfers between devices  5.1 us (3%)
    all_gather x1, blocking collectives, body(): lax.all_gather(over_z, 'y', axis=1, tiled=True).reshape(width, 3 * units)  61.7 us
    all_gather x1, blocking collectives, body(): over_z = lax.all_gather(shard, 'z', axis=0)  46.4 us
    all_to_all x1, blocking collectives, body(): parts = lax.all_to_all(paired, 'x', 0, 0)  25.1 us
    dot_general x2, matrix products, down_half(): lax.dot_general(mine, hidden, (((1,), (1,)), ((), ())), preferred_element...  6.78 us
    dot_general x2, matrix products, body(): jnp.dot(tokens, full[:, at:at + units].astype(jnp.bfloat16), preferred_el...  5.24 us
    ppermute x1, waiting for transfers between devices, body(): lax.ppermute(tails, ('z', 'y'), [(source, source + 1) for source in range...  4.76 us
  transfers between devices with their start and end apart: 2, of which 2 were waited for; matrix products, arithmetic and copies ran while one was open for 2% of the time, Pallas kernels for 0%

commit v1 on v0

--- a/solution.py
+++ b/solution.py
@@ -57,7 +57,9 @@
         [gate_weight * gain, value_weight * gain, down_weight.T * down_lift], axis=1
     ).astype(jnp.float16)
     over_z = lax.all_gather(shard, "z", axis=0)
-    full = lax.all_gather(over_z, "y", axis=1, tiled=True).reshape(width, 3 * units)
+    full = jnp.concatenate(
+        lax.all_to_all(jnp.stack([over_z] * lax.axis_size("y")), "y", 0, 0), axis=1
+    ).reshape(width, 3 * units)
     tokens, full = lax.optimization_barrier((tokens, full))
     values = tokens.astype(jnp.float32)
     factor = lax.rsqrt(jnp.mean(values * values, axis=1, keepdims=True) + epsilon) / up_lift

time: 164 us -> 200 us (1.22)
  blocking collectives: 133 us -> 158 us
  local copies, waits for them, and re-layouts: 1.31 us -> 7.02 us
  matrix products: 12 us -> 15.5 us
  other arithmetic: 6.59 us -> 8.63 us
    all_to_all x0 -> x1, blocking collectives: none -> 86 us  [body(): lax.all_to_all(jnp.stack([over_z] * lax.axis_size('y')), 'y', 0, 0)]
    all_gather x1 -> x0, blocking collectives: 61.7 us -> none  [body(): lax.all_gather(over_z, 'y', axis=1, tiled=True).reshape(width, 3 * units)]
    all_to_all x0 -> x1, local copies, waits for them, and re-layouts: none -> 4.92 us  [body(): lax.all_to_all(jnp.stack([over_z] * lax.axis_size('y')), 'y', 0, 0)]
    dot_general x2, matrix products: 5.24 us -> 8.75 us  [body(): jnp.dot(tokens, full[:, at:at + units].astype(jnp.bfloat16), preferred_el...]
    reduce_sum x1, other arithmetic: 0.68 us -> 2.72 us  [body(): jnp.mean(values * values, axis=1, keepdims=True) + epsilon]
  transfers between devices with their start and end apart: 2 -> 2, of which waited for: 2 -> 2; matrix products, arithmetic and copies ran while one was open for 2% -> 1% of each run, Pallas kernels for 0% -> 0%
where the time goes in v1:
time: 200 us; the launch traced here: 199 us
  blocking collectives  158 us (79%)
  matrix products  15.5 us (8%)
  other arithmetic  8.63 us (4%)
  local copies, waits for them, and re-layouts  7.02 us (4%)
  waiting for transfers between devices  5.85 us (3%)
  starting transfers between devices  4.38 us (2%)
    all_to_all x1, blocking collectives, body(): lax.all_to_all(jnp.stack([over_z] * lax.axis_size('y')), 'y', 0, 0)  86 us
    all_gather x1, blocking collectives, body(): over_z = lax.all_gather(shard, 'z', axis=0)  46.4 us
    all_to_all x1, blocking collectives, body(): parts = lax.all_to_all(paired, 'x', 0, 0)  25.1 us
    dot_general x2, matrix products, body(): jnp.dot(tokens, full[:, at:at + units].astype(jnp.bfloat16), preferred_el...  8.75 us
    dot_general x2, matrix products, down_half(): lax.dot_general(mine, hidden, (((1,), (1,)), ((), ())), preferred_element...  6.78 us
    ppermute x1, waiting for transfers between devices, body(): lax.ppermute(tails, ('z', 'y'), [(source, source + 1) for source in range...  5.06 us
    all_to_all x1, local copies, waits for them, and re-layouts, body(): lax.all_to_all(jnp.stack([over_z] * lax.axis_size('y')), 'y', 0, 0)  4.92 us
  transfers between devices with their start and end apart: 2, of which 2 were waited for; matrix products, arithmetic and copies ran while one was open for 1% of the time, Pallas kernels for 0%

profile of v1, /device:TPU:32, one launch (start us, length us, event | category | flops | bytes accessed | tf_op | source)
XLA Modules:
  0.0 199.1 jit_solution(8666482871790693275)
XLA Ops:
  0.0 0.9 fusion.37
  0.9 0.8 dynamic-slice_multiply_fusion
  1.7 1.0 fusion.35
  2.7 46.4 %all-gather.1 = f16[16,32,1920]{2,1,0:T(8,128)(2,1)S(1)} all-gather(f16[1,32,1920]{2,1,0:T(8,128)(2,1)S(1)} %pad_maximum_fusion), channel_id=1, replica_groups=mesh['z'=16,'y'=4,'x'=4,'c'=2] {'z'}, dimensions={0}, use_global_device_ids=true | all-gather | bytes 2088960 | tf_op jit(solution)/shard_map/all_gather | solution.py:59
  49.2 0.7 stack.2
  49.9 86.0 %all_to_all.10 = f16[4,16,32,1920]{3,2,1,0:T(8,128)(2,1)S(1)} all-to-all(f16[4,16,32,1920]{3,2,1,0:T(8,128)(2,1)S(1)} %stack.2), channel_id=1, replica_groups=mesh['z'=16,'y'=4,'x'=4,'c'=2] {'y'}, dimensions={0} | all-to-all | bytes 15728640 | tf_op jit(solution)/shard_map/all_to_all | solution.py:61
  135.8 4.9 %copy.15 = f16[4,16,32,1920]{3,2,0,1:T(8,128)(2,1)} copy(f16[4,16,32,1920]{3,2,1,0:T(8,128)(2,1)S(1)} %all_to_all.10) | data formatting | bytes 15728640 | tf_op jit(solution)/shard_map/all_to_all | solution.py:61
  140.8 2.7 %multiply_reduce_fusion = f32[768]{0:T(1024)S(1)} fusion(bf16[768,2048]{1,0:T(8,128)(2,1)} %param.12), kind=kLoop, calls=%fused_computation | loop fusion | flops 4717824 | bytes 3148800 | tf_op jit(solution)/shard_map/reduce_sum | solution.py:65
  143.5 0.1 copy-done
  143.6 0.0 copy-done.6
  143.6 4.4 %multiply_convert_fusion = bf16[768,640]{1,0:T(8,128)(2,1)S(1)} fusion(bf16[768,2048]{1,0:T(8,128)(2,1)S(1)} %copy-done, f16[2048,1920]{1,0:T(8,128)(2,1)} %bitcast.37, f32[640]{0:T(1024)S(1)} %copy-done.6, f32[768]{0:T(1024)S(1)} %rsqrt_multiply_fusion), kind=kOutput, calls=%fused_computation.31 | convolution fusion | flops 2016051200 | bytes 6755840 | tf_op jit(solution)/shard_map/dot_general | solution.py:68
  148.0 0.0 copy-done.7
  148.0 0.0 copy-start.1
  148.0 0.0 copy-start.2
  148.0 4.4 %multiply_convert_fusion.1 = bf16[768,640]{1,0:T(8,128)(2,1)S(1)} fusion(bf16[768,2048]{1,0:T(8,128)(2,1)S(1)} %copy-done, f16[2048,1920]{1,0:T(8,128)(2,1)} %bitcast.38, f32[640]{0:T(1024)S(1)} %copy-done.7, f32[768]{0:T(1024)S(1)} %rsqrt_multiply_fusion), kind=kOutput, calls=%fused_computation.32 | convolution fusion | flops 2016051200 | bytes 6755840 | tf_op jit(solution)/shard_map/dot_general | solution.py:68
  152.4 2.5 %collective-permute-start = (bf16[2,1280]{1,0:T(2,128)(2,1)S(1)}, bf16[2,1280]{1,0:T(2,128)(2,1)S(1)}, u32[]{:S(2)}, u32[]{:S(2)}) collective-permute-start(bf16[2,1280]{1,0:T(2,128)(2,1)S(1)} %pad_maximum_fusion.1), channel_id=1, source_target_pairs={{0,8},{8,16},{16,24},{24,32},{32,40},{40,48},{48,56},{56,64},{64,7... | collective-permute-start | bytes 15368 | tf_op jit(solution)/shard_map/ppermute | solution.py:75
  155.0 5.1 %collective-permute-done = bf16[2,1280]{1,0:T(2,128)(2,1)S(1)} collective-permute-done((bf16[2,1280]{1,0:T(2,128)(2,1)S(1)}, bf16[2,1280]{1,0:T(2,128)(2,1)S(1)}, u32[]{:S(2)}, u32[]{:S(2)}) %collective-permute-start) | collective-permute-done | bytes 5152 | tf_op jit(solution)/shard_map/ppermute | solution.py:75
  160.1 0.0 copy-start.4
  160.1 0.4 maximum_convert_fusion
  160.5 0.3 copy-done.3
  160.7 0.0 copy-done.4
  160.8 2.0 %fusion.14 = bf16[768,640]{1,0:T(8,128)(2,1)S(1)} fusion(f32[770,640]{1,0:T(8,128)S(1)} %get-tuple-element.24, f32[770,640]{1,0:T(8,128)S(1)} %get-tuple-element.23, f32[640]{0:T(1024)S(1)} %get-tuple-element.17, f32[640]{0:T(1024)S(1)} %get-tuple-element.18, f32[640]{0:T(1024)S(1)} %get-tuple-element.16, f32[640]{0:T(1024)S(1)} %copy-done.3, ...), kind=kLoop, calls=%fused_computation.18 | loop fusion | flops 10813440 | bytes 12800000 | tf_op jit(solution)/shard_map/convert_element_type | solution.py:80
  162.8 0.0 copy-start.5
  162.8 4.0 %convolution_convert_fusion = bf16[4,256,768]{2,1,0:T(8,128)(2,1)} fusion(f16[4,2,256,1920]{3,2,1,0:T(8,128)(2,1)} %bitcast.39, s32[]{:T(128)S(6)} %select_n.11, bf16[768,640]{1,0:T(8,128)(2,1)S(1)} %fusion.14), kind=kOutput, calls=%fused_computation.33 | convolution fusion | flops 1008074752 | bytes 3866628 | tf_op jit(solution)/shard_map/dot_general | solution.py:17
  166.8 1.9 collective-permute-start.1
  168.7 2.8 %fusion.28 = f32[4,256,768]{2,1,0:T(8,128)S(1)} fusion(f16[4,2,256,1920]{3,2,1,0:T(8,128)(2,1)} %bitcast.40, s32[]{:T(128)S(6)} %select_n.10, bf16[768,640]{1,0:T(8,128)(2,1)S(1)} %fusion.14), kind=kOutput, calls=%fused_computation.38 | convolution fusion | flops 1007288320 | bytes 5439492 | tf_op jit(solution)/shard_map/dot_general | solution.py:17
  171.5 0.8 collective-permute-done.1
  172.3 0.4 add_convert_fusion
  172.7 25.1 %all_to_all.11 = bf16[4,256,768]{2,1,0:T(8,128)(2,1)S(1)} all-to-all(bf16[4,256,768]{2,1,0:T(8,128)(2,1)S(1)} %add_convert_fusion), channel_id=1, replica_groups=mesh['z'=16,'y'=4,'x'=4,'c'=2] {'x'}, dimensions={0} | all-to-all | bytes 3145728 | tf_op jit(solution)/shard_map/all_to_all | solution.py:88
  197.8 0.2 convert_reduce_fusion
  198.1 0.1 fusion.34
  198.2 0.9 copy.18
  (15 shorter events, 0.1 us)
Async XLA Ops:
  140.7 2.8 %copy-start = (bf16[768,2048]{1,0:T(8,128)(2,1)S(1)}, bf16[768,2048]{1,0:T(8,128)(2,1)}, u32[]{:S(2)}) copy-start(bf16[768,2048]{1,0:T(8,128)(2,1)} %param.12) | copy-start | bytes 9437188
  140.7 2.8 %copy-start.6 = (f32[640]{0:T(1024)S(1)}, f32[640]{0:T(1024)}, u32[]{:S(2)}) copy-start(f32[640]{0:T(1024)} %param.17) | copy-start | bytes 7684
  143.6 4.4 %copy-start.7 = (f32[640]{0:T(1024)S(1)}, f32[640]{0:T(1024)}, u32[]{:S(2)}) copy-start(f32[640]{0:T(1024)} %param.16) | copy-start | bytes 7684
  148.0 6.9 %copy-start.1 = (f32[3,640]{1,0:T(4,128)S(1)}, f32[3,640]{1,0:T(4,128)}, u32[]{:S(2)}) copy-start(f32[3,640]{1,0:T(4,128)} %param.19) | copy-start | bytes 23044
  148.0 6.9 %copy-start.2 = (f32[3,640]{1,0:T(4,128)S(1)}, f32[3,640]{1,0:T(4,128)}, u32[]{:S(2)}) copy-start(f32[3,640]{1,0:T(4,128)} %param.18) | copy-start | bytes 23044
  152.4 7.6 %collective-permute-start = (bf16[2,1280]{1,0:T(2,128)(2,1)S(1)}, bf16[2,1280]{1,0:T(2,128)(2,1)S(1)}, u32[]{:S(2)}, u32[]{:S(2)}) collective-permute-start(bf16[2,1280]{1,0:T(2,128)(2,1)S(1)} %pad_maximum_fusion.1), channel_id=1, source_target_pairs={{0,8},{8,16},{16,24},{24,32},{32,40},{40,48},{48,56},{56,64},{64,7... | collective-permute-start | bytes 15368 | tf_op jit(solution)/shard_map/ppermute | solution.py:75
  160.1 0.7 copy-start.3
  160.1 0.7 copy-start.4
  162.8 5.9 %copy-start.5 = (f32[256]{0:T(256)S(1)}, f32[256]{0:T(256)}, u32[]{:S(2)}) copy-start(f32[256]{0:T(256)} %param.23) | copy-start | bytes 3076
  166.8 5.5 %collective-permute-start.1 = (bf16[4,256,768]{2,1,0:T(8,128)(2,1)}, bf16[4,256,768]{2,1,0:T(8,128)(2,1)S(1)}, u32[]{:S(2)}, u32[]{:S(2)}) collective-permute-start(bf16[4,256,768]{2,1,0:T(8,128)(2,1)} %convolution_convert_fusion), channel_id=1, source_target_pairs={{0,1},{1,0},{2,3},{3,2},{4,5},{5,4},{6,7},{7,6},{8,9},{9,8},{10,11... | collective-permute-start | bytes 4718600 | tf_op jit(solution)/shard_map/ppermute | solution.py:84
